TPU v7x, 32 devices: a whole 2x2x4 slice. The times are simulated.
32 devices in a mesh: sp: 8 (over z, x), tp: 4 (over y, core).
Axes of the slice: x: 2, y: 2, z: 4, core: 2. Of those that a mesh axis runs over, the one named last changes fastest.
Arguments:
- query_matrix: bfloat16 [2048, 1024], P('sp', 'tp'), may hold values from -6 to 6
- key_matrix: bfloat16 [2048, 1024], P('sp', 'tp'), may hold values from -6 to 6
- value_matrix: bfloat16 [2048, 2048], P('sp', 'tp'), may hold values from -6 to 6
- output_gate_rows: bfloat16 [2048, 2048], P('sp', 'tp'), may hold values from -6 to 6
- decay_preactivation: bfloat16 [2048, 1024], P('sp', 'tp'), may hold values from -5 to 5
- channel_decay_bias: float32 [1024], P('tp'), may hold values from 0 to 10
- extra_log_decay: float32 [2048, 16], P('sp', 'tp'), may hold values from -0.7 to 0
- head_norm_gain: float32 [128], replicated, may hold values from 0.1 to 1.9
- output_projection: bfloat16 [2048, 2048], P('tp'), may hold values from -0.125 to 0.125
- residual_input: bfloat16 [2048, 2048], P(('sp', 'tp')), may hold values from -6 to 6
- attention_norm_gain: float32 [2048], replicated, may hold values from 0.1 to 1.9
- expert_before_gain: float32 [2048], replicated, may hold values from 0.1 to 1.9
- expert_after_gain: float32 [2048], replicated, may hold values from 0.1 to 1.9
- expert_gate_weight: bfloat16 [8, 2048, 4096], P('sp', None, 'tp'), may hold values from -0.125 to 0.125
- expert_up_weight: bfloat16 [8, 2048, 4096], P('sp', None, 'tp'), may hold values from -0.125 to 0.125
- expert_down_weight: bfloat16 [8, 4096, 2048], P('sp', 'tp'), may hold values from -0.09375 to 0.09375
- token_expert_index: int32 [2048, 2], P('sp'), may hold values from 0 to 7, as said below
- routing_weight_matrix: float32 [2048, 2], P('sp'), may hold values from 0.1 to 1
Outputs:
- layer_out: bfloat16 [2048, 2048], P(('sp', 'tp'))
Inputs may be any that keep to these rules, and one draw needn't show every extreme that they name: `token_expert_index`: the 2 experts of a token differ and lie in one group: they have the same value of e // 4. In each aligned block of 256 rows (the rows of one index of sp) no expert is named by more than 80 rows, and the 4 experts of one group are each named by exactly 80 rows in every block.
All inputs are finite; a program needn't handle non-finite values.
Results may differ from a plain program's by a relative error of at most 0.024.
Values may be sent and summed in bfloat16 or wider, within the bound.
A program may use at most 64 MiB of HBM per device.

v0:
```python
import jax
import jax.numpy as jnp
from jax import lax
from jax.sharding import PartitionSpec as P

KEY_CHANNELS = 64
DV = 128
TOP = 2
BLOCK = 64


EPSILON = 1e-06
DECAY_NORMALIZER = 16.0
HIGHEST = lax.Precision.HIGHEST


def entering(shard, axis, join, neutral):
    place = lax.axis_index(axis)
    gathered = jax.tree.map(
        lambda a, kind: lax.all_gather(a.astype(kind), axis), shard, (jnp.bfloat16, jnp.bfloat16)
    )
    state = jax.tree.map(lambda a, e: jnp.zeros_like(a) + jnp.asarray(e, a.dtype), shard, neutral)

    def one(hop, state):
        return join(
            state,
            jax.tree.map(
                lambda a, own: lax.dynamic_index_in_dim(a, hop, 0, False).astype(own.dtype),
                gathered,
                shard,
            ),
        )

    return lax.fori_loop(0, place, one, state)


def rms_scale(values, gain_row):
    return (
        values * lax.rsqrt(jnp.mean(values * values, axis=-1, keepdims=True) + EPSILON) * gain_row
    )


def join_states(earlier, later):
    fade_one, state_one = earlier
    fade_two, state_two = later
    return (fade_one * fade_two, fade_two[..., None] * state_one + state_two)


def advance(running_state, inputs_pair):
    fade_now, grow_now = inputs_pair
    return (fade_now[..., None] * running_state + grow_now, running_state)


def shards(
    query_matrix,
    key_matrix,
    value_matrix,
    output_gate_rows,
    decay_preactivation,
    channel_decay_bias,
    extra_log_decay,
    head_norm_gain,
    output_projection,
    residual_input,
    attention_norm_gain,
    expert_before_gain,
    expert_after_gain,
    expert_gate_weight,
    expert_up_weight,
    expert_down_weight,
    token_expert_index,
    routing_weight_matrix,
):
    sequence_length = query_matrix.shape[0]
    number_heads = value_matrix.shape[1] // DV
    blocks = sequence_length // BLOCK
    queries = query_matrix.astype(jnp.float32).reshape(
        sequence_length, number_heads, KEY_CHANNELS
    ) * KEY_CHANNELS ** (-0.5)
    keys_all = key_matrix.astype(jnp.float32).reshape(sequence_length, number_heads, KEY_CHANNELS)
    values_all = value_matrix.astype(jnp.float32).reshape(sequence_length, number_heads, DV)
    decay_logarithm = (
        jax.nn.log_sigmoid(decay_preactivation.astype(jnp.float32) + channel_decay_bias)
        / DECAY_NORMALIZER
    )
    decay_logarithm = (
        decay_logarithm.reshape(sequence_length, number_heads, KEY_CHANNELS)
        + extra_log_decay[:, :, None]
    )
    running = jnp.cumsum(decay_logarithm, axis=0)
    total_fade = jnp.exp(running[-1])
    keys_to_end = keys_all * jnp.exp(running[-1] - running)
    total_growth = jnp.einsum("thd,thv->hdv", keys_to_end, values_all, precision=HIGHEST)
    q_blocks = queries.reshape(blocks, BLOCK, number_heads, KEY_CHANNELS)
    k_blocks = keys_all.reshape(blocks, BLOCK, number_heads, KEY_CHANNELS)
    v_blocks = values_all.reshape(blocks, BLOCK, number_heads, DV)
    inside = jnp.cumsum(decay_logarithm.reshape(blocks, BLOCK, number_heads, KEY_CHANNELS), axis=1)
    block_end = inside[:, -1:]
    q_decayed = q_blocks * jnp.exp(inside)
    k_inverse = k_blocks * jnp.exp(-inside)
    k_to_end = k_blocks * jnp.exp(block_end - inside)
    causal = jnp.tril(jnp.ones((BLOCK, BLOCK), dtype=bool))
    scores = jnp.einsum("nihd,njhd->nhij", q_decayed, k_inverse, precision=HIGHEST)
    scores = jnp.where(causal, scores, 0.0)
    within = jnp.einsum("nhij,njhv->nihv", scores, v_blocks, precision=HIGHEST)
    growth = jnp.einsum("nchd,nchv->nhdv", k_to_end, v_blocks, precision=HIGHEST)
    fade_rows = jnp.exp(block_end[:, 0])
    identity = (jnp.ones_like(total_fade), jnp.zeros_like(total_growth))
    _, carried = entering((total_fade, total_growth), "sp", join_states, identity)
    _, starts = lax.scan(advance, carried, (fade_rows, growth))
    across = jnp.einsum("nchd,nhdv->nchv", q_decayed, starts, precision=HIGHEST)
    attn = (within + across).reshape(sequence_length, number_heads, DV)
    gate_act = jax.nn.silu(
        output_gate_rows.astype(jnp.float32).reshape(sequence_length, number_heads, DV)
    )
    gated = (
        (rms_scale(attn, head_norm_gain) * gate_act)
        .astype(jnp.bfloat16)
        .reshape(sequence_length, number_heads * DV)
    )
    mixed = lax.psum_scatter(
        jnp.dot(gated, output_projection, preferred_element_type=jnp.float32).astype(jnp.bfloat16),
        "tp",
        scatter_dimension=0,
        tiled=True,
    ).astype(jnp.float32)
    layer_mid = (residual_input.astype(jnp.float32) + rms_scale(mixed, attention_norm_gain)).astype(
        jnp.bfloat16
    )
    normed = rms_scale(layer_mid.astype(jnp.float32), expert_before_gain).astype(jnp.bfloat16)
    block_rows = lax.all_gather(normed, "tp", axis=0, tiled=True)
    expert_count = lax.axis_size("sp")
    capacity = 5 * sequence_length // (2 * expert_count)
    flat_ids = token_expert_index.reshape(sequence_length * TOP)
    one_hot = (flat_ids[:, None] == jnp.arange(expert_count, dtype=jnp.int32)[None, :]).astype(
        jnp.int32
    )
    slot_index = jnp.sum((jnp.cumsum(one_hot, axis=0) - one_hot) * one_hot, axis=1)
    target = flat_ids * capacity + slot_index
    owners = jnp.zeros((expert_count * capacity,), jnp.int32)
    owners = owners.at[target].set(jnp.arange(sequence_length * TOP, dtype=jnp.int32) // TOP)
    owners = owners.reshape(expert_count, capacity)
    outgoing = block_rows[owners]
    arrived = lax.all_to_all(outgoing, "sp", split_axis=0, concat_axis=0, tiled=True)
    sources, slot_count, col_count = arrived.shape
    rows_in = arrived.reshape(sources * slot_count, col_count)
    gate_part = jnp.dot(rows_in, expert_gate_weight[0], preferred_element_type=jnp.float32)
    up_part = jnp.dot(rows_in, expert_up_weight[0], preferred_element_type=jnp.float32)
    hidden = (jax.nn.silu(gate_part) * up_part).astype(jnp.bfloat16)
    partial_value = jnp.dot(hidden, expert_down_weight[0], preferred_element_type=jnp.float32)
    partial_value = partial_value.reshape(sources, slot_count, col_count)
    share_part = lax.psum_scatter(
        partial_value.astype(jnp.bfloat16), "tp", scatter_dimension=2, tiled=True
    )
    back_rows = lax.all_to_all(share_part, "sp", split_axis=0, concat_axis=0, tiled=True)
    lookup = back_rows.reshape(expert_count * capacity, back_rows.shape[2])
    token_target = target.reshape(sequence_length, TOP)
    picked = lookup[token_target].astype(jnp.float32)
    column_sums = jnp.sum(routing_weight_matrix[:, :, None] * picked, axis=1)
    branch = lax.all_to_all(
        column_sums.astype(jnp.bfloat16), "tp", split_axis=0, concat_axis=1, tiled=True
    ).astype(column_sums.dtype)
    return (layer_mid.astype(jnp.float32) + rms_scale(branch, expert_after_gain)).astype(
        jnp.bfloat16
    )


def solution(mesh):
    placed = (
        P("sp", "tp"),
        P("sp", "tp"),
        P("sp", "tp"),
        P("sp", "tp"),
        P("sp", "tp"),
        P("tp"),
        P("sp", "tp"),
        P(),
        P("tp", None),
        P(("sp", "tp"), None),
        P(),
        P(),
        P(),
        P("sp", None, "tp"),
        P("sp", None, "tp"),
        P("sp", "tp", None),
        P("sp", None),
        P("sp", None),
    )
    return jax.shard_map(
        shards, mesh=mesh, in_specs=placed, out_specs=P(("sp", "tp"), None), check_vma=False
    )
```

profile of v0, /device:TPU:0, one launch (start us, length us, event | category | flops | bytes accessed | tf_op | source)
XLA Modules:
  0.0 304.3 jit_solution(13344771081159045010)
XLA Ops:
  6.5 1.2 copy.111
  11.9 1.4 fusion.30
  14.6 2.4 reduce-window.14
  18.1 1.2 copy.134
  22.0 1.2 exponential_multiply_fusion.1
  23.2 1.6 convolution_convert_fusion.1
  24.8 33.0 %all-gather = bf16[32,64,128]{2,1,0:T(8,128)(2,1)S(1)} all-gather(bf16[4,64,128]{2,1,0:T(8,128)(2,1)S(1)} %convolution_convert_fusion.1), channel_id=2, replica_groups=mesh['sp'=8,'tp'=4] {'sp'}, dimensions={0}, use_global_device_ids=true | all-gather | bytes 589824 | tf_op jit(solution)/shard_map/all_gather | solution.py:20
  57.8 21.7 %all_gather.13 = bf16[8,4,64]{2,1,0:T(4,128)(2,1)} all-gather(bf16[1,4,64]{2,1,0:T(4,128)(2,1)S(1)} %copy-done.7), channel_id=1, replica_groups=mesh['sp'=8,'tp'=4] {'sp'}, dimensions={0}, use_global_device_ids=true | all-gather | bytes 4608 | tf_op jit(solution)/shard_map/all_gather | solution.py:20
  79.5 2.0 reshape_reshape.6
  82.4 1.0 mul.178
  83.5 2.4 exponential_multiply_fusion
  86.5 3.2 %while.25 = (s32[]{:T(128)}, f32[4,64,128]{2,1,0:T(8,128)S(1)}, f32[4,4,64,128]{3,2,1,0:T(8,128)}, f32[4,4,64]{2,1,0:T(4,128)S(1)}, f32[4,4,64,128]{3,2,1,0:T(8,128)S(1)}, /*index=5*/s32[]{:T(128)}) while((s32[]{:T(128)}, f32[4,64,128]{2,1,0:T(8,128)S(1)}, f32[4,4,64,128]{3,2,1,0:T(8,128)}, f32[4,4,64]{2,1,0:T(4,128)S(1)}, ...), condition=%wide.region_6.7_spmd, body=%wide.region_5.6_spmd.sunk | while | flops 65538 | bytes 659021 | solution.py:110
  89.8 2.1 convolution_select_fusion
  94.0 1.8 convolution_convert_fusion
  95.8 27.0 %reduce-scatter.3.cloned.1.call-done = bf16[64,2048]{1,0:T(8,128)(2,1)} async-done(((bf16[256,2048]{1,0:T(8,128)(2,1)}), bf16[64,2048]{1,0:T(8,128)(2,1)}) %reduce-scatter.3.cloned.1.call-update) | async-done | bytes 262160 | tf_op jit(solution)/shard_map/reduce_scatter | solution.py:121
  122.8 1.1 fusion.16
  124.0 1.2 fusion.21
  126.6 1.1 reduce-window.16
  128.5 2.6 scatter_custom_fusion
  131.3 11.8 %all-gather.3.cloned.1.call-done = bf16[256,2048]{1,0:T(8,128)(2,1)} async-done(((bf16[64,2048]{1,0:T(8,128)(2,1)}), bf16[256,2048]{1,0:T(8,128)(2,1)}) %all-gather.3.cloned.1.call-update) | async-done | bytes 1048592 | tf_op jit(solution)/shard_map/all_gather | solution.py:131
  143.0 8.3 %gather_fusion = bf16[640,2048]{1,0:T(8,128)(2,1)} fusion(bf16[256,2048]{1,0:T(8,128)(2,1)} %all-gather.3.cloned.1.call-done, s32[1024]{0:T(1024)S(1)} %pad_clamp_fusion.1), kind=kCustom, calls=%fused_computation | custom fusion | bytes 5245440 | tf_op jit(solution)/shard_map/gather | solution.py:143
  151.3 65.6 %all_to_all.20 = bf16[8,80,2048]{2,1,0:T(8,128)(2,1)S(1)} all-to-all(bf16[8,80,2048]{2,1,0:T(8,128)(2,1)} %bitcast.120), channel_id=1, replica_groups=mesh['sp'=8,'tp'=4] {'sp'}, dimensions={0} | all-to-all | bytes 5242880 | tf_op jit(solution)/shard_map/all_to_all | solution.py:144
  216.9 2.9 fusion.2
  219.8 3.2 %multiply_convert_fusion = bf16[640,1024]{1,0:T(8,128)(2,1)S(1)} fusion(f32[640,1024]{1,0:T(8,128)S(1)} %fusion.2, bf16[640,2048]{1,0:T(8,128)(2,1)S(1)} %bitcast.122, bf16[1,2048,1024]{2,1,0:T(8,128)(2,1)S(1)} %copy-done.12), kind=kOutput, calls=%fused_computation.15 | convolution fusion | flops 2688286720 | bytes 10747904 | tf_op jit(solution)/shard_map/dot_general | solution.py:147
  223.1 4.2 %fusion.6 = bf16[8,80,2048]{2,1,0:T(8,128)(2,1)} fusion(bf16[8,80,1024]{2,1,0:T(8,128)(2,1)S(1)} %bitcast.135, bf16[1,1024,2048]{2,1,0:T(8,128)(2,1)S(1)} %copy-done.13), kind=kOutput, calls=%fused_computation.14 | convolution fusion | flops 2685665280 | bytes 8126464 | tf_op jit(solution)/shard_map/dot_general | solution.py:150
  227.3 32.7 %reduce-scatter.5.cloned.1.call-done = bf16[8,80,512]{2,1,0:T(8,128)(2,1)} async-done(((bf16[8,80,2048]{2,1,0:T(8,128)(2,1)}), bf16[8,80,512]{2,1,0:T(8,128)(2,1)}) %reduce-scatter.5.cloned.1.call-update) | async-done | bytes 655376 | tf_op jit(solution)/shard_map/reduce_scatter | solution.py:152
  259.9 5.5 %all-to-all-start.1 = ((bf16[8,80,512]{2,1,0:T(8,128)(2,1)}), bf16[8,80,512]{2,1,0:T(8,128)(2,1)S(1)}, u32[]{:S(2)}, u32[]{:S(2)}) async-start(bf16[8,80,512]{2,1,0:T(8,128)(2,1)} %reduce-scatter.5.cloned.1.call-done), calls=%async_computation.3 | async-start | bytes 1310720 | tf_op jit(solution)/shard_map/all_to_all | solution.py:155
  265.7 16.8 %all-to-all-done.1 = bf16[8,80,512]{2,1,0:T(8,128)(2,1)S(1)} async-done(((bf16[8,80,512]{2,1,0:T(8,128)(2,1)}), bf16[8,80,512]{2,1,0:T(8,128)(2,1)S(1)}, u32[]{:S(2)}, u32[]{:S(2)}) %all-to-all-start.1) | async-done | bytes 655392 | tf_op jit(solution)/shard_map/all_to_all | solution.py:155
  282.6 2.6 gather_fusion.1
  285.2 1.7 reshape.233
  286.9 1.3 multiply_reduce_fusion
  288.3 8.4 %all_to_all.21 = bf16[4,64,512]{2,1,0:T(8,128)(2,1)S(1)} all-to-all(bf16[4,64,512]{2,1,0:T(8,128)(2,1)S(1)} %bitcast.128), channel_id=1, replica_groups=mesh['sp'=8,'tp'=4] {'tp'}, dimensions={0} | all-to-all | bytes 524288 | tf_op jit(solution)/shard_map/all_to_all | solution.py:160
  (106 shorter events, 19.5 us)
Async XLA Ops:
  6.5 87.4 %copy-start = (bf16[512,2048]{1,0:T(8,128)(2,1)S(1)}, bf16[512,2048]{1,0:T(8,128)(2,1)}, u32[]{:S(2)}) copy-start(bf16[512,2048]{1,0:T(8,128)(2,1)} %param.30) | copy-start | bytes 6291460
  6.5 5.2 %copy-start.3 = (f32[256,4]{0,1:T(4,128)S(1)}, f32[256,4]{0,1:T(4,128)}, u32[]{:S(2)}) copy-start(f32[256,4]{0,1:T(4,128)} %param.28) | copy-start | bytes 12292
  6.5 116.3 %reduce-scatter.3.cloned.1.call-start = ((), (), s32[]{:S(2)}) async-start(), calls=%async_computation.5 | async-start | bytes 1310720 | tf_op jit(solution)/shard_map/reduce_scatter | solution.py:121
  22.0 35.8 %copy-start.7 = (bf16[1,4,64]{2,1,0:T(4,128)(2,1)S(1)}, bf16[1,4,64]{2,1,0:T(4,128)(2,1)}, u32[]{:S(2)}) copy-start(bf16[1,4,64]{2,1,0:T(4,128)(2,1)} %get-tuple-element.114) | copy-start | bytes 1540
  89.8 2.5 copy-start.1
  91.9 1.7 copy-start.10
  92.3 1.6 copy-start.14
  93.9 30.0 %copy-start.2 = (bf16[64,2048]{1,0:T(8,128)(2,1)S(1)}, bf16[64,2048]{1,0:T(8,128)(2,1)}, u32[]{:S(2)}) copy-start(bf16[64,2048]{1,0:T(8,128)(2,1)} %param.31) | copy-start | bytes 786436
  93.9 30.0 %copy-start.4 = (f32[2048]{0:T(1024)S(1)}, f32[2048]{0:T(1024)}, u32[]{:S(2)}) copy-start(f32[2048]{0:T(1024)} %param.32) | copy-start | bytes 24580
  93.9 31.3 %copy-start.5 = (f32[2048]{0:T(1024)S(1)}, f32[2048]{0:T(1024)}, u32[]{:S(2)}) copy-start(f32[2048]{0:T(1024)} %param.33) | copy-start | bytes 24580
  95.7 30.4 %copy-start.8 = (s32[256,2]{0,1:T(2,128)S(1)}, s32[256,2]{0,1:T(2,128)}, u32[]{:S(2)}) copy-start(s32[256,2]{0,1:T(2,128)} %param.38) | copy-start | bytes 6148
  95.8 47.3 %all-gather.3.cloned.1.call-start = ((), (), s32[]{:S(2)}) async-start(), calls=%async_computation.6 | async-start | bytes 1310720 | tf_op jit(solution)/shard_map/all_gather | solution.py:131
  126.1 133.8 %reduce-scatter.5.cloned.1.call-start = ((), (), s32[]{:S(2)}) async-start(), calls=%async_computation.7 | async-start | bytes 3276800 | tf_op jit(solution)/shard_map/reduce_scatter | solution.py:152
  151.3 65.6 %copy-start.11 = (bf16[1,2048,1024]{2,1,0:T(8,128)(2,1)S(1)}, bf16[1,2048,1024]{2,1,0:T(8,128)(2,1)}, u32[]{:S(2)}) copy-start(bf16[1,2048,1024]{2,1,0:T(8,128)(2,1)} %param.36) | copy-start | bytes 12582916
  216.9 2.9 copy-start.12
  219.8 3.3 %copy-start.13 = (bf16[1,1024,2048]{2,1,0:T(8,128)(2,1)S(1)}, bf16[1,1024,2048]{2,1,0:T(8,128)(2,1)}, u32[]{:S(2)}) copy-start(bf16[1,1024,2048]{2,1,0:T(8,128)(2,1)} %param.37) | copy-start | bytes 12582916
  227.2 38.3 %copy-start.9 = (f32[256,2]{0,1:T(2,128)S(1)}, f32[256,2]{0,1:T(2,128)}, u32[]{:S(2)}) copy-start(f32[256,2]{0,1:T(2,128)} %param.39) | copy-start | bytes 6148
  259.9 22.7 %all-to-all-start.1 = ((bf16[8,80,512]{2,1,0:T(8,128)(2,1)}), bf16[8,80,512]{2,1,0:T(8,128)(2,1)S(1)}, u32[]{:S(2)}, u32[]{:S(2)}) async-start(bf16[8,80,512]{2,1,0:T(8,128)(2,1)} %reduce-scatter.5.cloned.1.call-done), calls=%async_computation.3 | async-start | bytes 1310720 | tf_op jit(solution)/shard_map/all_to_all | solution.py:155
  285.2 11.7 %copy-start.6 = (f32[2048]{0:T(1024)S(1)}, f32[2048]{0:T(1024)}, u32[]{:S(2)}) copy-start(f32[2048]{0:T(1024)} %param.34) | copy-start | bytes 24580
Sparse Core Ops, SparseCore 0:
  95.9 26.9 reduce-scatter.2
  126.2 16.7 all-gather.2
  227.4 32.4 reduce-scatter.4
where the time goes:
time: 305 us; the launch traced here: 304 us
  blocking collectives  129 us (42%)
  waiting for transfers between devices  88.3 us (29%)
  local copies, waits for them, and re-layouts  31.6 us (10%)
  other arithmetic  18.9 us (6%)
  matrix products  17.4 us (6%)
  between operations  13.6 us (4%)
  starting transfers between devices  5.59 us (2%)
    all_to_all x1, blocking collectives, shards(): lax.all_to_all(outgoing, 'sp', split_axis=0, concat_axis=0, tiled=True)  65.6 us
    all_gather x2, blocking collectives, entering(): lax.all_gather(a.astype(kind), axis)  54.7 us
    reduce_scatter x1, waiting for transfers between devices, shards(): lax.psum_scatter(partial_value.astype(jnp.bfloat16), 'tp', scatter_dimens...  32.7 us
    reduce_scatter x1, waiting for transfers between devices, shards(): lax.psum_scatter(jnp.dot(gated, output_projection, preferred_element_type...  27 us
    all_to_all x1, waiting for transfers between devices, shards(): lax.all_to_all(share_part, 'sp', split_axis=0, concat_axis=0, tiled=True)  16.8 us
    all_gather x1, waiting for transfers between devices, shards(): block_rows = lax.all_gather(normed, 'tp', axis=0, tiled=True)  11.8 us
    all_to_all x1, blocking collectives, shards(): lax.all_to_all(column_sums.astype(jnp.bfloat16), 'tp', split_axis=0, conc...  8.39 us
    gather x1, local copies, waits for them, and re-layouts, shards(): outgoing = block_rows[owners]  8.28 us
  transfers between devices with their start and end apart: 4, of which 4 were waited for; matrix products, arithmetic and copies ran while one was open for 2% of the time, Pallas kernels for 0%

commit v1 on v0

v1 whole, which is shorter than its diff:
```python
import functools

import jax
import jax.numpy as jnp
from jax import lax
from jax.experimental import pallas as pl
from jax.experimental.pallas import tpu as pltpu
from jax.sharding import PartitionSpec as P

KEY_CHANNELS = 64
DV = 128
TOP = 2
BLOCK = 64

EPSILON = 1e-06
DECAY_NORMALIZER = 16.0
HIGHEST = lax.Precision.HIGHEST
MESH = pl.DeviceIdType.MESH
F32 = jnp.float32
BF16 = jnp.bfloat16
FADE_ROWS = 16


def rms_scale(values, gain_row):
    return (
        values * lax.rsqrt(jnp.mean(values * values, axis=-1, keepdims=True) + EPSILON) * gain_row
    )


def contract(a, b, da, db):
    return lax.dot_general(a, b, (((da,), (db,)), ((), ())), preferred_element_type=F32)


def loop(count, body):
    def step(i, carry):
        body(i)
        return carry

    lax.fori_loop(0, count, step, 0)


def remote(src, dst, send, recv, device):
    return pltpu.make_async_remote_copy(
        src_ref=src,
        dst_ref=dst,
        send_sem=send,
        recv_sem=recv,
        device_id=device,
        device_id_type=MESH,
    )


def attention_kernel(
    n_sp, q_ref, k_ref, v_ref, g_ref, d_ref, bias_ref, extra_ref, hgain_ref, w_ref,
    out_ref, message, inbox, carried, gated, send_sem, recv_sem,
):
    me = lax.axis_index("sp")
    barrier = pltpu.get_barrier_semaphore()

    def greet(i):
        @pl.when(me - 1 - i >= 0)
        def _():
            pl.semaphore_signal(
                barrier, inc=1, device_id={"sp": jnp.maximum(me - 1 - i, 0)}, device_id_type=MESH
            )

    loop(n_sp - 1, greet)

    length, width = q_ref.shape
    heads = width // KEY_CHANNELS
    blocks = length // BLOCK
    x = d_ref[...].astype(F32) + bias_ref[...]
    log_decay = (jnp.minimum(x, 0.0) - jnp.log1p(jnp.exp(-jnp.abs(x)))) / DECAY_NORMALIZER
    extra = extra_ref[...]
    log_decay = log_decay + jnp.concatenate(
        [jnp.broadcast_to(extra[:, h : h + 1], (length, KEY_CHANNELS)) for h in range(heads)],
        axis=1,
    )
    row = lax.broadcasted_iota(jnp.int32, (length, length), 0)
    col = lax.broadcasted_iota(jnp.int32, (length, length), 1)
    causal = (row >= col) & (row // BLOCK == col // BLOCK)
    inside = jnp.dot(
        jnp.where(causal, 1.0, 0.0).astype(F32), log_decay, precision=HIGHEST,
        preferred_element_type=F32,
    )
    ends = [inside[(b + 1) * BLOCK - 1 : (b + 1) * BLOCK, :] for b in range(blocks)]
    offsets = [jnp.zeros_like(ends[0])]
    for b in range(blocks):
        offsets.append(offsets[-1] + ends[b])

    def spread(rows):
        return jnp.concatenate([jnp.broadcast_to(r, (BLOCK, width)) for r in rows], axis=0)

    q = q_ref[...].astype(F32) * KEY_CHANNELS ** (-0.5)
    k = k_ref[...].astype(F32)
    k_end = (k * jnp.exp(spread(ends) - inside)).astype(BF16)
    states = [jnp.zeros((DV, width), F32)]
    for b in range(blocks):
        rows = slice(b * BLOCK, (b + 1) * BLOCK)
        grown = jnp.concatenate(
            [
                contract(
                    v_ref[rows, h * DV : (h + 1) * DV],
                    k_end[rows, h * KEY_CHANNELS : (h + 1) * KEY_CHANNELS],
                    0,
                    0,
                )
                for h in range(heads)
            ],
            axis=1,
        )
        states.append(states[-1] * jnp.exp(ends[b]) + grown)
    message[0:DV, :] = states[-1].astype(BF16)
    message[DV:, :] = jnp.broadcast_to(jnp.exp(offsets[-1]), (FADE_ROWS, width)).astype(BF16)

    @pl.when(me < n_sp - 1)
    def _():
        pl.semaphore_wait(barrier, n_sp - 1 - me)

    def copy_of(i):
        return remote(
            message, inbox.at[me], send_sem.at[i], recv_sem.at[me],
            {"sp": jnp.minimum(me + 1 + i, n_sp - 1)},
        )

    def send(i):
        @pl.when(me + 1 + i < n_sp)
        def _():
            copy_of(i).start()

    loop(n_sp - 1, send)

    q_in = (q * jnp.exp(inside)).astype(BF16)
    k_inv = (k * jnp.exp(-inside)).astype(BF16)
    q_all = (q * jnp.exp(inside + spread(offsets[:-1]))).astype(BF16)
    local = []
    for h in range(heads):
        cs = slice(h * KEY_CHANNELS, (h + 1) * KEY_CHANNELS)
        scores = jnp.where(causal, contract(q_in[:, cs], k_inv[:, cs], 1, 1), 0.0).astype(BF16)
        within = jnp.dot(scores, v_ref[:, h * DV : (h + 1) * DV], preferred_element_type=F32)
        across = jnp.concatenate(
            [jnp.zeros((BLOCK, DV), F32)]
            + [
                contract(
                    q_in[b * BLOCK : (b + 1) * BLOCK, cs], states[b][:, cs].astype(BF16), 1, 1
                )
                for b in range(1, blocks)
            ],
            axis=0,
        )
        local.append(within + across)

    carried[...] = jnp.zeros_like(carried)

    def take(hop):
        @pl.when(hop < me)
        def _():
            remote(
                message, inbox.at[hop], send_sem.at[0], recv_sem.at[hop], {"sp": me}
            ).wait_recv()
            carried[...] = carried[...] * inbox[hop, DV : DV + 1, :].astype(F32) + inbox[
                hop, 0:DV, :
            ].astype(F32)

    loop(n_sp - 1, take)

    start = carried[...].astype(BF16)
    for h in range(heads):
        cs = slice(h * KEY_CHANNELS, (h + 1) * KEY_CHANNELS)
        vs = slice(h * DV, (h + 1) * DV)
        attn = local[h] + contract(q_all[:, cs], start[:, cs], 1, 1)
        gate = g_ref[:, vs].astype(F32)
        gated[:, vs] = (rms_scale(attn, hgain_ref[...]) * (gate * jax.nn.sigmoid(gate))).astype(
            BF16
        )
    out_ref[...] = jnp.dot(gated[...], w_ref[...], preferred_element_type=F32).astype(BF16)

    def drain(i):
        @pl.when(me + 1 + i < n_sp)
        def _():
            copy_of(i).wait_send()

    loop(n_sp - 1, drain)


def greet_all(n_sp, n_tp, me, j):
    barrier = pltpu.get_barrier_semaphore()

    def along_sp(i):
        pl.semaphore_signal(
            barrier, inc=1, device_id={"sp": lax.rem(me + 1 + i, n_sp)}, device_id_type=MESH
        )

    def along_tp(i):
        pl.semaphore_signal(
            barrier, inc=1, device_id={"tp": lax.rem(j + 1 + i, n_tp)}, device_id_type=MESH
        )

    loop(n_sp - 1, along_sp)
    loop(n_tp - 1, along_tp)
    pl.semaphore_wait(barrier, n_sp + n_tp - 2)


def dispatch_kernel(
    n_sp, n_tp, cap, part_ref, res_ref, again_ref, bgain_ref, target_ref,
    mid_ref, rows_ref,
    ra, rb, tb, normed, xcol, outgoing,
    sa, va, sb, vb, st, vt, ss, vs, sy, vy, sd, vd,
):
    me = lax.axis_index("sp")
    j = lax.axis_index("tp")
    n_y = n_tp // 2
    y, c = j // 2, lax.rem(j, 2)
    sibling = 2 * y + 1 - c
    rows = res_ref.shape[0]
    share = part_ref.shape[1] // n_tp
    greet_all(n_sp, n_tp, me, j)

    def rows_of(index):
        return pl.ds(pl.multiple_of(index * rows, rows), rows)

    def cols_of(index):
        return pl.ds(pl.multiple_of(index * share, share), share)

    def y_at(i):
        return lax.rem(y + 1 + i, n_y)

    def y_from(i):
        return lax.rem(y + n_y - 1 - i, n_y)

    def pair_copy(i):
        return remote(
            part_ref.at[rows_of(2 * y_at(i) + 1 - c)], ra.at[i], sa.at[i], va.at[i],
            {"tp": sibling},
        )

    def far_copy(i):
        return remote(tb.at[i], rb.at[i], sb.at[i], vb.at[i], {"tp": 2 * y_at(i) + c})

    loop(n_y, lambda i: pair_copy(i).start())

    def pair_sum(i):
        pair_copy(i).wait_recv()
        tb[i] = (
            part_ref[rows_of(2 * y_at(i) + c), :].astype(F32) + ra[i].astype(F32)
        ).astype(BF16)
        far_copy(i).start()

    loop(n_y - 1, pair_sum)
    pair_copy(n_y - 1).wait_recv()
    mixed = part_ref[rows_of(j), :].astype(F32) + ra[n_y - 1].astype(F32)
    for i in range(n_y - 1):
        far_copy(i).wait_recv()
        mixed = mixed + rb[i].astype(F32)
    mid = (res_ref[...].astype(F32) + rms_scale(mixed, again_ref[...])).astype(BF16)
    mid_ref[...] = mid
    normed[...] = rms_scale(mid.astype(F32), bgain_ref[...]).astype(BF16)

    def turn_copy(i):
        peer = lax.rem(j + 1 + i, n_tp)
        return remote(
            normed.at[:, cols_of(peer)], xcol.at[rows_of(j)], st.at[i], vt.at[i], {"tp": peer}
        )

    loop(n_tp - 1, lambda i: turn_copy(i).start())
    xcol[rows_of(j), :] = normed[:, cols_of(j)]
    loop(n_tp - 1, lambda i: turn_copy(i).wait_recv())

    x = xcol[...]
    t0, t1 = target_ref[0:1, :], target_ref[1:2, :]
    tokens = x.shape[0]

    def picked(expert):
        slot = lax.broadcasted_iota(jnp.int32, (cap, tokens), 0) + expert * cap
        chosen = jnp.where((slot == t0) | (slot == t1), 1.0, 0.0).astype(BF16)
        return jnp.dot(chosen, x, preferred_element_type=F32).astype(BF16)

    def out_copy(i):
        return remote(
            outgoing.at[i], rows_ref.at[me, :, cols_of(j)], ss.at[i], vs.at[i],
            {"sp": lax.rem(me + 1 + i, n_sp)},
        )

    def send(i):
        outgoing[i] = picked(lax.rem(me + 1 + i, n_sp))
        out_copy(i).start()

    loop(n_sp - 1, send)
    rows_ref[me, :, cols_of(j)] = picked(me)

    def source(i):
        return lax.rem(me + n_sp - i, n_sp)

    def y_copy(i, m):
        place = rows_ref.at[source(i), :, cols_of(j)]
        return remote(place, place, sy.at[m, i], vy.at[m, i], {"tp": 2 * y_at(m) + c})

    def pair_forward(i, m, owner):
        place = rows_ref.at[source(i), :, cols_of(owner)]
        return remote(place, place, sd.at[m, i], vd.at[m, i], {"tp": sibling})

    def arrived(i):
        @pl.when(i > 0)
        def _():
            out_copy(jnp.maximum(i - 1, 0)).wait_recv()

        for m in range(n_y - 1):
            y_copy(i, m).start()
        pair_forward(i, n_y - 1, j).start()

    loop(n_sp, arrived)

    def relay(i):
        for m in range(n_y - 1):
            y_copy(i, m).wait_recv()
            pair_forward(i, m, 2 * y_from(m) + c).start()

    loop(n_sp, relay)

    def finish(i):
        for m in range(n_y - 1):
            pair_forward(i, m, 2 * y_from(m) + c).wait()
            y_copy(i, m).wait_send()
        pair_forward(i, n_y - 1, j).wait()

    loop(n_sp, finish)

    def drain_pair(i):
        pair_copy(i).wait_send()

    loop(n_y, drain_pair)
    loop(n_y - 1, lambda i: far_copy(i).wait_send())
    loop(n_tp - 1, lambda i: turn_copy(i).wait_send())
    loop(n_sp - 1, lambda i: out_copy(i).wait_send())


def combine_kernel(
    n_sp, n_tp, cap, p_ref, mid_ref, gain_ref, target_ref, weight_ref,
    out_ref,
    r1, r2, tb, ob, back, turned, brow,
    s1, v1, s2, v2, s3, v3, s4, v4,
):
    me = lax.axis_index("sp")
    j = lax.axis_index("tp")
    n_y = n_tp // 2
    y, c = j // 2, lax.rem(j, 2)
    sibling = 2 * y + 1 - c
    rows = mid_ref.shape[0]
    share = p_ref.shape[2] // n_tp
    greet_all(n_sp, n_tp, me, j)

    def rows_of(index):
        return pl.ds(pl.multiple_of(index * rows, rows), rows)

    def cols_of(index):
        return pl.ds(pl.multiple_of(index * share, share), share)

    def y_at(i):
        return lax.rem(y + 1 + i, n_y)

    def block_of(i):
        return lax.rem(me + 1 + i, n_sp)

    def pair_copy(i, m):
        return remote(
            p_ref.at[block_of(i), :, cols_of(2 * y_at(m) + 1 - c)], r1.at[i, m],
            s1.at[i, m], v1.at[i, m], {"tp": sibling},
        )

    def far_copy(i, m):
        return remote(
            tb.at[i, m], r2.at[i, m], s2.at[i, m], v2.at[i, m], {"tp": 2 * y_at(m) + c}
        )

    def back_copy(i):
        return remote(ob.at[i], back.at[me], s3.at[i], v3.at[i], {"sp": block_of(i)})

    def first(i):
        for m in range(n_y):
            pair_copy(i, m).start()

    loop(n_sp, first)

    def second(i):
        for m in range(n_y - 1):
            pair_copy(i, m).wait_recv()
            tb[i, m] = (
                p_ref[block_of(i), :, cols_of(2 * y_at(m) + c)].astype(F32)
                + r1[i, m].astype(F32)
            ).astype(BF16)
            far_copy(i, m).start()

    loop(n_sp, second)

    def summed(i):
        pair_copy(i, n_y - 1).wait_recv()
        total = p_ref[block_of(i), :, cols_of(j)].astype(F32) + r1[i, n_y - 1].astype(F32)
        for m in range(n_y - 1):
            far_copy(i, m).wait_recv()
            total = total + r2[i, m].astype(F32)
        return total.astype(BF16)

    def third(i):
        ob[i] = summed(i)
        back_copy(i).start()

    loop(n_sp - 1, third)
    back[me] = summed(n_sp - 1)

    tokens = target_ref.shape[0]
    t0, t1 = target_ref[:, 0:1], target_ref[:, 1:2]
    w0, w1 = weight_ref[:, 0:1], weight_ref[:, 1:2]

    def weighed(expert):
        slot = lax.broadcasted_iota(jnp.int32, (tokens, cap), 1) + expert * cap
        mix = jnp.where(slot == t0, w0, 0.0) + jnp.where(slot == t1, w1, 0.0)
        high = mix.astype(BF16)
        low = (mix - high.astype(F32)).astype(BF16)
        served = back[expert]
        return jnp.dot(high, served, preferred_element_type=F32) + jnp.dot(
            low, served, preferred_element_type=F32
        )

    def gather(i, total):
        back_copy(i).wait_recv()
        return total + weighed(lax.rem(me + n_sp - 1 - i, n_sp))

    turned[...] = lax.fori_loop(0, n_sp - 1, gather, weighed(me)).astype(BF16)

    def turn_copy(i):
        peer = lax.rem(j + 1 + i, n_tp)
        return remote(
            turned.at[rows_of(peer)], brow.at[:, cols_of(j)], s4.at[i], v4.at[i], {"tp": peer}
        )

    loop(n_tp - 1, lambda i: turn_copy(i).start())
    brow[:, cols_of(j)] = turned[rows_of(j), :]
    loop(n_tp - 1, lambda i: turn_copy(i).wait_recv())
    out_ref[...] = (
        mid_ref[...].astype(F32) + rms_scale(brow[...].astype(F32), gain_ref[...])
    ).astype(BF16)

    def drain(i):
        for m in range(n_y):
            pair_copy(i, m).wait_send()
        for m in range(n_y - 1):
            far_copy(i, m).wait_send()

    loop(n_sp, drain)
    loop(n_sp - 1, lambda i: back_copy(i).wait_send())
    loop(n_tp - 1, lambda i: turn_copy(i).wait_send())


def call(kernel, operands, outs, scratch, ident, limit=48 << 20):
    vmem = pl.BlockSpec(memory_space=pltpu.VMEM)
    return pl.pallas_call(
        kernel,
        out_shape=outs,
        in_specs=[vmem] * len(operands),
        out_specs=jax.tree.map(lambda _: vmem, outs),
        scratch_shapes=scratch,
        compiler_params=pltpu.CompilerParams(
            collective_id=ident, has_side_effects=True, vmem_limit_bytes=limit
        ),
    )(*operands)


def dmas(*shapes):
    return [pltpu.SemaphoreType.DMA(s) for s in shapes]


def shards(
    n_sp,
    n_tp,
    query_matrix,
    key_matrix,
    value_matrix,
    output_gate_rows,
    decay_preactivation,
    channel_decay_bias,
    extra_log_decay,
    head_norm_gain,
    output_projection,
    residual_input,
    attention_norm_gain,
    expert_before_gain,
    expert_after_gain,
    expert_gate_weight,
    expert_up_weight,
    expert_down_weight,
    token_expert_index,
    routing_weight_matrix,
):
    length, width = query_matrix.shape
    model = output_projection.shape[1]
    rows = residual_input.shape[0]
    share = model // n_tp
    n_y = n_tp // 2
    capacity = 5 * length // (2 * n_sp)
    cap = (capacity + 15) // 16 * 16
    values = value_matrix.shape[1]

    flat = token_expert_index.reshape(length * TOP)
    one_hot = flat[:, None] == jnp.arange(n_sp, dtype=jnp.int32)[None, :]
    order = jnp.arange(length * TOP, dtype=jnp.int32)
    earlier = (order[:, None] > order[None, :]).astype(BF16)
    counts = jnp.dot(earlier, one_hot.astype(BF16), preferred_element_type=F32)
    slot = jnp.sum(jnp.where(one_hot, counts, 0.0), axis=1).astype(jnp.int32)
    target = (flat * cap + slot).reshape(length, TOP)

    part = call(
        functools.partial(attention_kernel, n_sp),
        (
            query_matrix,
            key_matrix,
            value_matrix,
            output_gate_rows,
            decay_preactivation,
            channel_decay_bias.reshape(1, width),
            extra_log_decay,
            head_norm_gain.reshape(1, DV),
            output_projection,
        ),
        jax.ShapeDtypeStruct((length, model), BF16),
        [
            pltpu.VMEM((DV + FADE_ROWS, width), BF16),
            pltpu.VMEM((n_sp, DV + FADE_ROWS, width), BF16),
            pltpu.VMEM((DV, width), F32),
            pltpu.VMEM((length, values), BF16),
        ]
        + dmas((n_sp,), (n_sp,)),
        1,
    )
    mid, rows_in = call(
        functools.partial(dispatch_kernel, n_sp, n_tp, cap),
        (
            part,
            residual_input,
            attention_norm_gain.reshape(1, model),
            expert_before_gain.reshape(1, model),
            target.T,
        ),
        (
            jax.ShapeDtypeStruct((rows, model), BF16),
            jax.ShapeDtypeStruct((n_sp, cap, model), BF16),
        ),
        [
            pltpu.VMEM((n_y, rows, model), BF16),
            pltpu.VMEM((n_y, rows, model), BF16),
            pltpu.VMEM((n_y, rows, model), BF16),
            pltpu.VMEM((rows, model), BF16),
            pltpu.VMEM((length, share), BF16),
            pltpu.VMEM((n_sp, cap, share), BF16),
        ]
        + dmas(
            (n_y,), (n_y,), (n_y,), (n_y,), (n_tp,), (n_tp,), (n_sp,), (n_sp,),
            (n_y, n_sp), (n_y, n_sp), (n_y, n_sp), (n_y, n_sp),
        ),
        2,
    )
    rows_in = rows_in.reshape(n_sp * cap, model)
    gate_part = jnp.dot(rows_in, expert_gate_weight[0], preferred_element_type=F32)
    up_part = jnp.dot(rows_in, expert_up_weight[0], preferred_element_type=F32)
    hidden = (jax.nn.silu(gate_part) * up_part).astype(BF16)
    partial_value = jnp.dot(hidden, expert_down_weight[0], preferred_element_type=F32)
    partial_value = partial_value.astype(BF16).reshape(n_sp, cap, model)
    return call(
        functools.partial(combine_kernel, n_sp, n_tp, cap),
        (
            partial_value,
            mid,
            expert_after_gain.reshape(1, model),
            target,
            routing_weight_matrix,
        ),
        jax.ShapeDtypeStruct((rows, model), BF16),
        [
            pltpu.VMEM((n_sp, n_y, cap, share), BF16),
            pltpu.VMEM((n_sp, n_y, cap, share), BF16),
            pltpu.VMEM((n_sp, n_y, cap, share), BF16),
            pltpu.VMEM((n_sp, cap, share), BF16),
            pltpu.VMEM((n_sp, cap, share), BF16),
            pltpu.VMEM((length, share), BF16),
            pltpu.VMEM((rows, model), BF16),
        ]
        + dmas(
            (n_sp, n_y), (n_sp, n_y), (n_sp, n_y), (n_sp, n_y), (n_sp,), (n_sp,), (n_tp,), (n_tp,)
        ),
        3,
    )


def solution(mesh):
    placed = (
        P("sp", "tp"),
        P("sp", "tp"),
        P("sp", "tp"),
        P("sp", "tp"),
        P("sp", "tp"),
        P("tp"),
        P("sp", "tp"),
        P(),
        P("tp", None),
        P(("sp", "tp"), None),
        P(),
        P(),
        P(),
        P("sp", None, "tp"),
        P("sp", None, "tp"),
        P("sp", "tp", None),
        P("sp", None),
        P("sp", None),
    )
    return jax.shard_map(
        functools.partial(shards, mesh.shape["sp"], mesh.shape["tp"]),
        mesh=mesh,
        in_specs=placed,
        out_specs=P(("sp", "tp"), None),
        check_vma=False,
    )
```

time: 305 us -> 121 us (0.40)
  blocking collectives: 129 us -> 0 us
  Pallas kernels: 0 us -> 92.1 us
  waiting for transfers between devices: 88.3 us -> 0 us
  local copies, waits for them, and re-layouts: 31.6 us -> 12 us
  other arithmetic: 18.9 us -> 0.71 us
  between operations: 13.6 us -> 0.19 us
  starting transfers between devices: 5.59 us -> 0 us
    pallas_call x0 -> x3, Pallas kernels: none -> 92.1 us  [call(): pl.pallas_call(kernel, out_shape=outs, in_specs=[vmem] * len(operands), o...]
    all_to_all x2 -> x0, blocking collectives: 74 us -> none  [the longest x1 65.6 us: shards(): lax.all_to_all(outgoing, 'sp', split_axis=0, concat_axis=0, tiled=True)]
    reduce_scatter x2 -> x0, waiting for transfers between devices: 59.7 us -> none  [the longest x1 32.7 us: shards(): lax.psum_scatter(partial_value.astype(jnp.bfloat16), 'tp', scatter_dimens...]
    all_gather x2 -> x0, blocking collectives: 54.7 us -> none  [entering(): lax.all_gather(a.astype(kind), axis)]
    all_to_all x1 -> x0, waiting for transfers between devices: 16.8 us -> none  [shards(): lax.all_to_all(share_part, 'sp', split_axis=0, concat_axis=0, tiled=True)]
    all_gather x1 -> x0, waiting for transfers between devices: 11.8 us -> none  [shards(): block_rows = lax.all_gather(normed, 'tp', axis=0, tiled=True)]
    gather x2 -> x0, local copies, waits for them, and re-layouts: 10.9 us -> none  [the longest x1 8.28 us: shards(): outgoing = block_rows[owners]]
    unnamed x34, local copies, waits for them, and re-layouts: 2.5 us -> 11.5 us
  transfers between devices with their start and end apart: 4 -> 0, of which waited for: 4 -> 0; matrix products, arithmetic and copies ran while one was open for 2% -> 0% of each run, Pallas kernels for 0% -> 0%
where the time goes in v1:
time: 121 us
  Pallas kernels  92.1 us (76%)
  matrix products  15.4 us (13%)
  local copies, waits for them, and re-layouts  12 us (10%)
    pallas_call x3, Pallas kernels, call(): pl.pallas_call(kernel, out_shape=outs, in_specs=[vmem] * len(operands), o...  92.1 us
    unnamed x34, local copies, waits for them, and re-layouts  11.5 us
    dot_general x1, matrix products, shards(): jnp.dot(hidden, expert_down_weight[0], preferred_element_type=F32)  10.8 us
    dot_general x1, matrix products, shards(): up_part = jnp.dot(rows_in, expert_up_weight[0], preferred_element_type=F32)  4.38 us

profile of v1, /device:TPU:0, one launch (start us, length us, event | category | flops | bytes accessed | tf_op | source)
XLA Modules:
  0.0 120.5 jit_solution(16813480597433643612)
XLA Ops:
  0.0 0.8 copy.31
  0.8 0.1 eq.15
  1.0 0.3 fusion.11
  1.2 0.0 copy-start.3
  1.2 0.0 copy-start.8
  1.3 0.0 copy-start.9
  1.3 0.1 convert_element_type.16
  1.4 0.7 broadcast_multiply_fusion
  2.1 0.1 copy.32
  2.3 0.1 copy.33.target_ref
  2.4 0.8 copy.30.extra_ref
  3.2 0.0 copy-start
  3.2 1.6 %copy-done = bf16[512,2048]{1,0:T(8,128)(2,1)S(1)} copy-done((bf16[512,2048]{1,0:T(8,128)(2,1)S(1)}, bf16[512,2048]{1,0:T(8,128)(2,1)}, u32[]{:S(2)}) %copy-start) | copy-done | bytes 2097176
  4.8 0.9 copy-done.1
  5.7 0.9 copy-done.2
  6.7 0.9 copy-done.4
  7.6 0.9 copy-done.5
  8.5 0.9 copy-done.6
  9.4 0.7 copy-done.10
  10.1 0.7 copy-done.11
  10.7 15.6 %shard_map.172.part_ref = bf16[256,2048]{1,0:T(8,128)(2,1)S(1)} custom-call(bf16[256,256]{1,0:T(8,128)(2,1)S(1)} %copy-done.4, bf16[256,256]{1,0:T(8,128)(2,1)S(1)} %copy-done.5, bf16[256,512]{1,0:T(8,128)(2,1)S(1)} %copy-done.1, bf16[256,512]{1,0:T(8,128)(2,1)S(1)} %copy-done.2, bf16[256,256]{1,0:T(8,128)(2,1)S(1)} %copy-done.6, f32[1,256]{1,0:T(1,128)S(1)} %bitcast.30, ...), custom_call_target="tpu_custom_call" | custom-call | tf_op jit(solution)/shard_map/pallas_call | solution.py:456
  26.4 0.0 copy-done.3
  26.4 0.0 copy-done.8
  26.4 45.1 %shard_map.173 = (bf16[64,2048]{1,0:T(8,128)(2,1)S(1)}, bf16[8,80,2048]{2,1,0:T(8,128)(2,1)S(1)}) custom-call(bf16[256,2048]{1,0:T(8,128)(2,1)S(1)} %shard_map.172.part_ref, bf16[64,2048]{1,0:T(8,128)(2,1)S(1)} %copy-done.3, f32[1,2048]{1,0:T(1,128)S(1)} %bitcast.28, f32[1,2048]{1,0:T(1,128)S(1)} %bitcast.29, s32[2,256]{1,0:T(2,128)S(1)} %copy.33.target_ref), custom_call_target="tpu_custom_call" | custom-call | tf_op jit(solution)/shard_map/pallas_call | solution.py:456
  71.5 0.0 copy-start.12
  71.5 1.5 %copy-done.12 = bf16[8,80,2048]{2,1,0:T(8,128)(2,1)} copy-done((bf16[8,80,2048]{2,1,0:T(8,128)(2,1)}, bf16[8,80,2048]{2,1,0:T(8,128)(2,1)S(1)}, u32[]{:S(2)}) %copy-start.12) | copy-done | bytes 2621464
  73.0 0.0 copy-done.14
  73.0 4.4 %fusion.2 = f32[640,1024]{1,0:T(8,128)} fusion(bf16[640,2048]{1,0:T(8,128)(2,1)S(1)} %bitcast.32, bf16[1,2048,1024]{2,1,0:T(8,128)(2,1)S(1)} %copy-done.14), kind=kOutput, calls=%fused_computation.2 | convolution fusion | flops 2684354560 | bytes 9437184 | tf_op jit(solution)/shard_map/dot_general | solution.py:563
  77.4 10.8 %fusion.6 = bf16[640,2048]{1,0:T(8,128)(2,1)S(1)} fusion(bf16[1,1024,2048]{2,1,0:T(8,128)(2,1)} %param.33, f32[640,1024]{1,0:T(8,128)} %fusion.2, bf16[640,2048]{1,0:T(8,128)(2,1)} %bitcast.33, bf16[1,2048,1024]{2,1,0:T(8,128)(2,1)} %param.31), kind=kOutput, calls=%fused_computation.6 | convolution fusion | flops 5373952000 | bytes 16252928 | tf_op jit(solution)/shard_map/dot_general | solution.py:565
  88.2 0.1 copy.34.weight_ref
  88.4 31.4 %shard_map.174 = bf16[64,2048]{1,0:T(8,128)(2,1)S(1)} custom-call(bf16[8,80,2048]{2,1,0:T(8,128)(2,1)S(1)} %bitcast.25, bf16[64,2048]{1,0:T(8,128)(2,1)S(1)} %get-tuple-element.8.mid_ref, f32[1,2048]{1,0:T(1,128)S(1)} %bitcast.27, s32[256,2]{1,0:T(8,128)S(1)} %add.8.target_ref, f32[256,2]{1,0:T(8,128)S(1)} %copy.34.weight_ref), custom_call_target="tpu_custom_call" | custom-call | tf_op jit(solution)/shard_map/pallas_call | solution.py:456
  119.8 0.7 copy.36
  (15 shorter events, 0.0 us)
Async XLA Ops:
  1.2 25.1 %copy-start.3 = (bf16[64,2048]{1,0:T(8,128)(2,1)S(1)}, bf16[64,2048]{1,0:T(8,128)(2,1)}, u32[]{:S(2)}) copy-start(bf16[64,2048]{1,0:T(8,128)(2,1)} %res_ref.1) | copy-start | bytes 786436
  1.2 25.1 %copy-start.8 = (f32[2048]{0:T(1024)S(1)}, f32[2048]{0:T(1024)}, u32[]{:S(2)}) copy-start(f32[2048]{0:T(1024)} %param.28) | copy-start | bytes 24580
  1.3 25.1 %copy-start.9 = (f32[2048]{0:T(1024)S(1)}, f32[2048]{0:T(1024)}, u32[]{:S(2)}) copy-start(f32[2048]{0:T(1024)} %param.29) | copy-start | bytes 24580
  3.2 1.6 %copy-start = (bf16[512,2048]{1,0:T(8,128)(2,1)S(1)}, bf16[512,2048]{1,0:T(8,128)(2,1)}, u32[]{:S(2)}) copy-start(bf16[512,2048]{1,0:T(8,128)(2,1)} %w_ref.1) | copy-start | bytes 6291460
  4.8 0.9 copy-start.1
  5.7 0.9 copy-start.2
  6.7 0.9 copy-start.4
  7.6 0.9 copy-start.5
  8.5 0.9 copy-start.6
  9.4 0.7 copy-start.10
  10.1 0.7 copy-start.11
  10.7 62.3 %copy-start.14 = (bf16[1,2048,1024]{2,1,0:T(8,128)(2,1)S(1)}, bf16[1,2048,1024]{2,1,0:T(8,128)(2,1)}, u32[]{:S(2)}) copy-start(bf16[1,2048,1024]{2,1,0:T(8,128)(2,1)} %param.32) | copy-start | bytes 12582916
  71.5 1.5 %copy-start.12 = (bf16[8,80,2048]{2,1,0:T(8,128)(2,1)}, bf16[8,80,2048]{2,1,0:T(8,128)(2,1)S(1)}, u32[]{:S(2)}) copy-start(bf16[8,80,2048]{2,1,0:T(8,128)(2,1)S(1)} %get-tuple-element.7) | copy-start | bytes 7864324
  77.4 10.8 %copy-start.13 = (f32[256,2]{0,1:T(2,128)S(1)}, f32[256,2]{0,1:T(2,128)}, u32[]{:S(2)}) copy-start(f32[256,2]{0,1:T(2,128)} %param.35) | copy-start | bytes 6148
  77.4 11.0 %copy-start.7 = (f32[2048]{0:T(1024)S(1)}, f32[2048]{0:T(1024)}, u32[]{:S(2)}) copy-start(f32[2048]{0:T(1024)} %param.30) | copy-start | bytes 24580

commit v2 on v1

--- a/solution.py
+++ b/solution.py
@@ -51,10 +51,26 @@
 
 
 def attention_kernel(
-    n_sp, q_ref, k_ref, v_ref, g_ref, d_ref, bias_ref, extra_ref, hgain_ref, w_ref,
-    out_ref, message, inbox, carried, gated, send_sem, recv_sem,
+    n_sp, q_hbm, k_hbm, v_hbm, g_hbm, d_hbm, bias_ref, extra_ref, hgain_ref, w_hbm,
+    out_ref, message, inbox, carried, gated, q_ref, k_ref, v_ref, g_ref, d_ref, w_ref,
+    send_sem, recv_sem, load_sem,
 ):
     me = lax.axis_index("sp")
+    loads = [
+        pltpu.make_async_copy(src, dst, load_sem.at[n])
+        for n, (src, dst) in enumerate(
+            (
+                (d_hbm, d_ref),
+                (k_hbm, k_ref),
+                (v_hbm, v_ref),
+                (q_hbm, q_ref),
+                (g_hbm, g_ref),
+                (w_hbm, w_ref),
+            )
+        )
+    ]
+    for copy in loads:
+        copy.start()
     barrier = pltpu.get_barrier_semaphore()
 
     def greet(i):
@@ -66,6 +82,7 @@
 
     loop(n_sp - 1, greet)
 
+    loads[0].wait()
     length, width = q_ref.shape
     heads = width // KEY_CHANNELS
     blocks = length // BLOCK
@@ -91,6 +108,8 @@
     def spread(rows):
         return jnp.concatenate([jnp.broadcast_to(r, (BLOCK, width)) for r in rows], axis=0)
 
+    for copy in loads[1:4]:
+        copy.wait()
     q = q_ref[...].astype(F32) * KEY_CHANNELS ** (-0.5)
     k = k_ref[...].astype(F32)
     k_end = (k * jnp.exp(spread(ends) - inside)).astype(BF16)
@@ -164,6 +183,8 @@
 
     loop(n_sp - 1, take)
 
+    for copy in loads[4:]:
+        copy.wait()
     start = carried[...].astype(BF16)
     for h in range(heads):
         cs = slice(h * KEY_CHANNELS, (h + 1) * KEY_CHANNELS)
@@ -201,19 +222,38 @@
     pl.semaphore_wait(barrier, n_sp + n_tp - 2)
 
 
-def dispatch_kernel(
-    n_sp, n_tp, cap, part_ref, res_ref, again_ref, bgain_ref, target_ref,
-    mid_ref, rows_ref,
-    ra, rb, tb, normed, xcol, outgoing,
-    sa, va, sb, vb, st, vt, ss, vs, sy, vy, sd, vd,
+def flipped(me, i, n):
+    total, bit = 0, 1
+    while bit < n:
+        total = total + lax.rem(me // bit + i // bit, 2) * bit
+        bit *= 2
+    return total
+
+
+def expert_kernel(
+    n_sp, n_tp, cap, part_ref, res_hbm, again_ref, bgain_ref, fgain_ref, target_ref, turned_ref,
+    weight_ref, wg_hbm, wu_hbm, wd_hbm,
+    out_ref,
+    res_ref, wg, wu, wd, ra, rb, tb, normed, xcol, outgoing, rows_ref, hidden, p_ref,
+    r1, r2, ty, ob, back, branch, brow, mid_ref,
+    load, sa, va, sb, vb, st, vt, ss, vs, sy, vy, sd, vd, s1, v1, s2, v2, s3, v3, s4, v4,
 ):
     me = lax.axis_index("sp")
     j = lax.axis_index("tp")
     n_y = n_tp // 2
     y, c = j // 2, lax.rem(j, 2)
     sibling = 2 * y + 1 - c
-    rows = res_ref.shape[0]
-    share = part_ref.shape[1] // n_tp
+    rows, model = res_ref.shape
+    share = model // n_tp
+    half = n_sp // 2
+    loads = [
+        pltpu.make_async_copy(src, dst, load.at[n])
+        for n, (src, dst) in enumerate(
+            ((res_hbm, res_ref), (wg_hbm, wg), (wu_hbm, wu), (wd_hbm, wd))
+        )
+    ]
+    for copy in loads:
+        copy.start()
     greet_all(n_sp, n_tp, me, j)
 
     def rows_of(index):
@@ -228,29 +268,33 @@
     def y_from(i):
         return lax.rem(y + n_y - 1 - i, n_y)
 
-    def pair_copy(i):
+    def peer_of(i):
+        return flipped(me, i, n_sp)
+
+    def head_pair(i):
         return remote(
             part_ref.at[rows_of(2 * y_at(i) + 1 - c)], ra.at[i], sa.at[i], va.at[i],
             {"tp": sibling},
         )
 
-    def far_copy(i):
+    def head_far(i):
         return remote(tb.at[i], rb.at[i], sb.at[i], vb.at[i], {"tp": 2 * y_at(i) + c})
 
-    loop(n_y, lambda i: pair_copy(i).start())
+    loop(n_y, lambda i: head_pair(i).start())
 
     def pair_sum(i):
-        pair_copy(i).wait_recv()
+        head_pair(i).wait_recv()
         tb[i] = (
             part_ref[rows_of(2 * y_at(i) + c), :].astype(F32) + ra[i].astype(F32)
         ).astype(BF16)
-        far_copy(i).start()
+        head_far(i).start()
 
     loop(n_y - 1, pair_sum)
-    pair_copy(n_y - 1).wait_recv()
+    head_pair(n_y - 1).wait_recv()
     mixed = part_ref[rows_of(j), :].astype(F32) + ra[n_y - 1].astype(F32)
+    loads[0].wait()
     for i in range(n_y - 1):
-        far_copy(i).wait_recv()
+        head_far(i).wait_recv()
         mixed = mixed + rb[i].astype(F32)
     mid = (res_ref[...].astype(F32) + rms_scale(mixed, again_ref[...])).astype(BF16)
     mid_ref[...] = mid
@@ -267,7 +311,7 @@
     loop(n_tp - 1, lambda i: turn_copy(i).wait_recv())
 
     x = xcol[...]
-    t0, t1 = target_ref[0:1, :], target_ref[1:2, :]
+    t0, t1 = turned_ref[0:1, :], turned_ref[1:2, :]
     tokens = x.shape[0]
 
     def picked(expert):
@@ -278,142 +322,148 @@
     def out_copy(i):
         return remote(
             outgoing.at[i], rows_ref.at[me, :, cols_of(j)], ss.at[i], vs.at[i],
-            {"sp": lax.rem(me + 1 + i, n_sp)},
+            {"sp": peer_of(i)},
         )
 
     def send(i):
-        outgoing[i] = picked(lax.rem(me + 1 + i, n_sp))
-        out_copy(i).start()
+        outgoing[i + 1] = picked(peer_of(i + 1))
+        out_copy(i + 1).start()
 
     loop(n_sp - 1, send)
     rows_ref[me, :, cols_of(j)] = picked(me)
 
-    def source(i):
-        return lax.rem(me + n_sp - i, n_sp)
-
     def y_copy(i, m):
-        place = rows_ref.at[source(i), :, cols_of(j)]
+        place = rows_ref.at[peer_of(i), :, cols_of(j)]
         return remote(place, place, sy.at[m, i], vy.at[m, i], {"tp": 2 * y_at(m) + c})
 
     def pair_forward(i, m, owner):
-        place = rows_ref.at[source(i), :, cols_of(owner)]
+        place = rows_ref.at[peer_of(i), :, cols_of(owner)]
         return remote(place, place, sd.at[m, i], vd.at[m, i], {"tp": sibling})
 
-    def arrived(i):
-        @pl.when(i > 0)
-        def _():
-            out_copy(jnp.maximum(i - 1, 0)).wait_recv()
-
+    def forward(i):
         for m in range(n_y - 1):
             y_copy(i, m).start()
         pair_forward(i, n_y - 1, j).start()
 
-    loop(n_sp, arrived)
+    def arrived(i):
+        out_copy(i).wait_recv()
+        forward(i)
 
     def relay(i):
         for m in range(n_y - 1):
             y_copy(i, m).wait_recv()
             pair_forward(i, m, 2 * y_from(m) + c).start()
 
-    loop(n_sp, relay)
-
-    def finish(i):
+    def ready(i):
         for m in range(n_y - 1):
-            pair_forward(i, m, 2 * y_from(m) + c).wait()
-            y_copy(i, m).wait_send()
-        pair_forward(i, n_y - 1, j).wait()
-
-    loop(n_sp, finish)
-
-    def drain_pair(i):
-        pair_copy(i).wait_send()
-
-    loop(n_y, drain_pair)
-    loop(n_y - 1, lambda i: far_copy(i).wait_send())
-    loop(n_tp - 1, lambda i: turn_copy(i).wait_send())
-    loop(n_sp - 1, lambda i: out_copy(i).wait_send())
-
-
-def combine_kernel(
-    n_sp, n_tp, cap, p_ref, mid_ref, gain_ref, target_ref, weight_ref,
-    out_ref,
-    r1, r2, tb, ob, back, turned, brow,
-    s1, v1, s2, v2, s3, v3, s4, v4,
-):
-    me = lax.axis_index("sp")
-    j = lax.axis_index("tp")
-    n_y = n_tp // 2
-    y, c = j // 2, lax.rem(j, 2)
-    sibling = 2 * y + 1 - c
-    rows = mid_ref.shape[0]
-    share = p_ref.shape[2] // n_tp
-    greet_all(n_sp, n_tp, me, j)
-
-    def rows_of(index):
-        return pl.ds(pl.multiple_of(index * rows, rows), rows)
-
-    def cols_of(index):
-        return pl.ds(pl.multiple_of(index * share, share), share)
-
-    def y_at(i):
-        return lax.rem(y + 1 + i, n_y)
-
-    def block_of(i):
-        return lax.rem(me + 1 + i, n_sp)
-
-    def pair_copy(i, m):
+            pair_forward(i, m, 2 * y_from(m) + c).wait_recv()
+        pair_forward(i, n_y - 1, j).wait_recv()
+
+    def part_pair(i, m):
         return remote(
-            p_ref.at[block_of(i), :, cols_of(2 * y_at(m) + 1 - c)], r1.at[i, m],
+            p_ref.at[peer_of(i), :, cols_of(2 * y_at(m) + 1 - c)], r1.at[i, m],
             s1.at[i, m], v1.at[i, m], {"tp": sibling},
         )
 
-    def far_copy(i, m):
+    def part_far(i, m):
         return remote(
-            tb.at[i, m], r2.at[i, m], s2.at[i, m], v2.at[i, m], {"tp": 2 * y_at(m) + c}
+            ty.at[i, m], r2.at[i, m], s2.at[i, m], v2.at[i, m], {"tp": 2 * y_at(m) + c}
         )
 
     def back_copy(i):
-        return remote(ob.at[i], back.at[me], s3.at[i], v3.at[i], {"sp": block_of(i)})
-
-    def first(i):
-        for m in range(n_y):
-            pair_copy(i, m).start()
-
-    loop(n_sp, first)
-
-    def second(i):
+        return remote(ob.at[i], back.at[me], s3.at[i], v3.at[i], {"sp": peer_of(i)})
+
+    def pass_along(i, m):
+        part_pair(i, m).wait_recv()
+        ty[i, m] = (
+            p_ref[peer_of(i), :, cols_of(2 * y_at(m) + c)].astype(F32) + r1[i, m].astype(F32)
+        ).astype(BF16)
+        part_far(i, m).start()
+
+    def summed(i):
+        part_pair(i, n_y - 1).wait_recv()
+        total = p_ref[peer_of(i), :, cols_of(j)].astype(F32) + r1[i, n_y - 1].astype(F32)
         for m in range(n_y - 1):
-            pair_copy(i, m).wait_recv()
-            tb[i, m] = (
-                p_ref[block_of(i), :, cols_of(2 * y_at(m) + c)].astype(F32)
-                + r1[i, m].astype(F32)
-            ).astype(BF16)
-            far_copy(i, m).start()
-
-    loop(n_sp, second)
-
-    def summed(i):
-        pair_copy(i, n_y - 1).wait_recv()
-        total = p_ref[block_of(i), :, cols_of(j)].astype(F32) + r1[i, n_y - 1].astype(F32)
-        for m in range(n_y - 1):
-            far_copy(i, m).wait_recv()
+            part_far(i, m).wait_recv()
             total = total + r2[i, m].astype(F32)
         return total.astype(BF16)
 
-    def third(i):
+    def give_back(i):
         ob[i] = summed(i)
         back_copy(i).start()
 
-    loop(n_sp - 1, third)
-    back[me] = summed(n_sp - 1)
-
-    tokens = target_ref.shape[0]
-    t0, t1 = target_ref[:, 0:1], target_ref[:, 1:2]
+    tile = min(256, wg.shape[1])
+    steps = wg.shape[1] // tile
+
+    def run_expert(first, during_up, during_down):
+        blocks = pl.ds(peer_of(first) // half * half, half)
+        batch = half * cap
+
+        def up(t):
+            cols = pl.ds(pl.multiple_of(t * tile, tile), tile)
+            fed = rows_ref[blocks].reshape(batch, model)
+            gate = jnp.dot(fed, wg[:, cols], preferred_element_type=F32)
+            rise = jnp.dot(fed, wu[:, cols], preferred_element_type=F32)
+            hidden[:, cols] = (gate * jax.nn.sigmoid(gate) * rise).astype(BF16)
+            during_up(t)
+
+        loop(steps, up)
+
+        def down(owner):
+            made = jnp.dot(hidden[...], wd[:, cols_of(owner)], preferred_element_type=F32)
+            p_ref[blocks, :, cols_of(owner)] = made.astype(BF16).reshape(half, cap, share)
+
+        def down_pair(m):
+            down(2 * y_at(m) + 1 - c)
+            loop(half, lambda i: part_pair(first + i, m).start())
+            during_down(m)
+            down(2 * y_at(m) + c)
+
+            @pl.when(m < n_y - 1)
+            def _():
+                loop(half, lambda i: pass_along(first + i, m))
+
+        loop(n_y, down_pair)
+
+    def spaced(count, parts, body):
+        each = -(-count // parts)
+
+        def hook(t):
+            def one(i):
+                @pl.when(t * each + i < count)
+                def _():
+                    body(jnp.minimum(t * each + i, count - 1))
+
+            loop(each, one)
+
+        return hook
+
+    forward(0)
+    loop(half - 1, lambda i: arrived(i + 1))
+    loop(half, relay)
+    loop(half, ready)
+    for copy in loads[1:]:
+        copy.wait()
+    run_expert(
+        0,
+        spaced(half, steps, lambda i: arrived(half + i)),
+        spaced(half, n_y, lambda i: relay(half + i)),
+    )
+    loop(half, lambda i: ready(half + i))
+    run_expert(
+        half,
+        spaced(half - 1, steps, lambda i: give_back(i + 1)),
+        lambda m: None,
+    )
+    loop(half, lambda i: give_back(half + i))
+    back[me] = summed(0)
+
+    u0, u1 = target_ref[:, 0:1], target_ref[:, 1:2]
     w0, w1 = weight_ref[:, 0:1], weight_ref[:, 1:2]
 
     def weighed(expert):
         slot = lax.broadcasted_iota(jnp.int32, (tokens, cap), 1) + expert * cap
-        mix = jnp.where(slot == t0, w0, 0.0) + jnp.where(slot == t1, w1, 0.0)
+        mix = jnp.where(slot == u0, w0, 0.0) + jnp.where(slot == u1, w1, 0.0)
         high = mix.astype(BF16)
         low = (mix - high.astype(F32)).astype(BF16)
         served = back[expert]
@@ -423,40 +473,54 @@
 
     def gather(i, total):
         back_copy(i).wait_recv()
-        return total + weighed(lax.rem(me + n_sp - 1 - i, n_sp))
-
-    turned[...] = lax.fori_loop(0, n_sp - 1, gather, weighed(me)).astype(BF16)
-
-    def turn_copy(i):
+        return total + weighed(peer_of(i))
+
+    branch[...] = lax.fori_loop(1, n_sp, gather, weighed(me)).astype(BF16)
+
+    def home_copy(i):
         peer = lax.rem(j + 1 + i, n_tp)
         return remote(
-            turned.at[rows_of(peer)], brow.at[:, cols_of(j)], s4.at[i], v4.at[i], {"tp": peer}
-        )
-
-    loop(n_tp - 1, lambda i: turn_copy(i).start())
-    brow[:, cols_of(j)] = turned[rows_of(j), :]
-    loop(n_tp - 1, lambda i: turn_copy(i).wait_recv())
+            branch.at[rows_of(peer)], brow.at[:, cols_of(j)], s4.at[i], v4.at[i], {"tp": peer}
+        )
+
+    loop(n_tp - 1, lambda i: home_copy(i).start())
+    brow[:, cols_of(j)] = branch[rows_of(j), :]
+    loop(n_tp - 1, lambda i: home_copy(i).wait_recv())
     out_ref[...] = (
-        mid_ref[...].astype(F32) + rms_scale(brow[...].astype(F32), gain_ref[...])
+        mid_ref[...].astype(F32) + rms_scale(brow[...].astype(F32), fgain_ref[...])
     ).astype(BF16)
 
+    loop(n_y, lambda i: head_pair(i).wait_send())
+    loop(n_y - 1, lambda i: head_far(i).wait_send())
+    loop(n_sp - 1, lambda i: out_copy(i + 1).wait_send())
+    loop(n_sp - 1, lambda i: back_copy(i + 1).wait_send())
+
+    def drain_turns(i):
+        turn_copy(i).wait_send()
+        home_copy(i).wait_send()
+
+    loop(n_tp - 1, drain_turns)
+
     def drain(i):
+        for m in range(n_y - 1):
+            y_copy(i, m).wait_send()
+            pair_forward(i, m, 2 * y_from(m) + c).wait_send()
+            part_far(i, m).wait_send()
+        pair_forward(i, n_y - 1, j).wait_send()
         for m in range(n_y):
-            pair_copy(i, m).wait_send()
-        for m in range(n_y - 1):
-            far_copy(i, m).wait_send()
+            part_pair(i, m).wait_send()
 
     loop(n_sp, drain)
-    loop(n_sp - 1, lambda i: back_copy(i).wait_send())
-    loop(n_tp - 1, lambda i: turn_copy(i).wait_send())
-
-
-def call(kernel, operands, outs, scratch, ident, limit=48 << 20):
+
+
+def call(kernel, operands, far, outs, scratch, ident, limit):
     vmem = pl.BlockSpec(memory_space=pltpu.VMEM)
     return pl.pallas_call(
         kernel,
         out_shape=outs,
-        in_specs=[vmem] * len(operands),
+        in_specs=[
+            pl.BlockSpec(memory_space=pl.ANY) if n in far else vmem for n in range(len(operands))
+        ],
         out_specs=jax.tree.map(lambda _: vmem, outs),
         scratch_shapes=scratch,
         compiler_params=pltpu.CompilerParams(
@@ -521,72 +585,73 @@
             head_norm_gain.reshape(1, DV),
             output_projection,
         ),
+        (0, 1, 2, 3, 4, 8),
         jax.ShapeDtypeStruct((length, model), BF16),
         [
             pltpu.VMEM((DV + FADE_ROWS, width), BF16),
             pltpu.VMEM((n_sp, DV + FADE_ROWS, width), BF16),
             pltpu.VMEM((DV, width), F32),
             pltpu.VMEM((length, values), BF16),
+            pltpu.VMEM((length, width), BF16),
+            pltpu.VMEM((length, width), BF16),
+            pltpu.VMEM((length, values), BF16),
+            pltpu.VMEM((length, values), BF16),
+            pltpu.VMEM((length, width), BF16),
+            pltpu.VMEM((values, model), BF16),
         ]
-        + dmas((n_sp,), (n_sp,)),
+        + dmas((n_sp,), (n_sp,), (6,)),
         1,
-    )
-    mid, rows_in = call(
-        functools.partial(dispatch_kernel, n_sp, n_tp, cap),
+        32 << 20,
+    )
+    hidden_units = expert_gate_weight.shape[2]
+    by_peer = (n_sp, n_y)
+    return call(
+        functools.partial(expert_kernel, n_sp, n_tp, cap),
         (
             part,
             residual_input,
             attention_norm_gain.reshape(1, model),
             expert_before_gain.reshape(1, model),
+            expert_after_gain.reshape(1, model),
+            target,
             target.T,
+            routing_weight_matrix,
+            expert_gate_weight[0],
+            expert_up_weight[0],
+            expert_down_weight[0],
         ),
-        (
-            jax.ShapeDtypeStruct((rows, model), BF16),
-            jax.ShapeDtypeStruct((n_sp, cap, model), BF16),
-        ),
+        (1, 8, 9, 10),
+        jax.ShapeDtypeStruct((rows, model), BF16),
         [
+            pltpu.VMEM((rows, model), BF16),
+            pltpu.VMEM((model, hidden_units), BF16),
+            pltpu.VMEM((model, hidden_units), BF16),
+            pltpu.VMEM((hidden_units, model), BF16),
             pltpu.VMEM((n_y, rows, model), BF16),
             pltpu.VMEM((n_y, rows, model), BF16),
             pltpu.VMEM((n_y, rows, model), BF16),
             pltpu.VMEM((rows, model), BF16),
             pltpu.VMEM((length, share), BF16),
             pltpu.VMEM((n_sp, cap, share), BF16),
-        ]
-        + dmas(
-            (n_y,), (n_y,), (n_y,), (n_y,), (n_tp,), (n_tp,), (n_sp,), (n_sp,),
-            (n_y, n_sp), (n_y, n_sp), (n_y, n_sp), (n_y, n_sp),
-        ),
-        2,
-    )
-    rows_in = rows_in.reshape(n_sp * cap, model)
-    gate_part = jnp.dot(rows_in, expert_gate_weight[0], preferred_element_type=F32)
-    up_part = jnp.dot(rows_in, expert_up_weight[0], preferred_element_type=F32)
-    hidden = (jax.nn.silu(gate_part) * up_part).astype(BF16)
-    partial_value = jnp.dot(hidden, expert_down_weight[0], preferred_element_type=F32)
-    partial_value = partial_value.astype(BF16).reshape(n_sp, cap, model)
-    return call(
-        functools.partial(combine_kernel, n_sp, n_tp, cap),
-        (
-            partial_value,
-            mid,
-            expert_after_gain.reshape(1, model),
-            target,
-            routing_weight_matrix,
-        ),
-        jax.ShapeDtypeStruct((rows, model), BF16),
-        [
-            pltpu.VMEM((n_sp, n_y, cap, share), BF16),
-            pltpu.VMEM((n_sp, n_y, cap, share), BF16),
-            pltpu.VMEM((n_sp, n_y, cap, share), BF16),
+            pltpu.VMEM((n_sp, cap, model), BF16),
+            pltpu.VMEM((n_sp // 2 * cap, hidden_units), BF16),
+            pltpu.VMEM((n_sp, cap, model), BF16),
+            pltpu.VMEM(by_peer + (cap, share), BF16),
+            pltpu.VMEM(by_peer + (cap, share), BF16),
+            pltpu.VMEM(by_peer + (cap, share), BF16),
             pltpu.VMEM((n_sp, cap, share), BF16),
             pltpu.VMEM((n_sp, cap, share), BF16),
             pltpu.VMEM((length, share), BF16),
             pltpu.VMEM((rows, model), BF16),
+            pltpu.VMEM((rows, model), BF16),
         ]
         + dmas(
-            (n_sp, n_y), (n_sp, n_y), (n_sp, n_y), (n_sp, n_y), (n_sp,), (n_sp,), (n_tp,), (n_tp,)
+            (4,), (n_y,), (n_y,), (n_y,), (n_y,), (n_tp,), (n_tp,), (n_sp,), (n_sp,),
+            (n_y, n_sp), (n_y, n_sp), (n_y, n_sp), (n_y, n_sp),
+            by_peer, by_peer, by_peer, by_peer, (n_sp,), (n_sp,), (n_tp,), (n_tp,),
         ),
-        3,
+        2,
+        56 << 20,
     )
 
 

time: 121 us -> 111 us (0.917)
  matrix products: 15.4 us -> 0.26 us
  local copies, waits for them, and re-layouts: 12 us -> 14.4 us
  Pallas kernels: 92.1 us -> 94.2 us
    dot_general x2 -> x0, matrix products: 15.2 us -> none  [the longest x1 10.8 us: shards(): jnp.dot(hidden, expert_down_weight[0], preferred_element_type=F32)]
    pallas_call x3 -> x2, Pallas kernels: 92.1 us -> 94.2 us  [call(): pl.pallas_call(kernel, out_shape=outs, in_specs=[pl.BlockSpec(memory_spac...]
    unnamed x34 -> x24, local copies, waits for them, and re-layouts: 11.5 us -> 13.3 us
where the time goes in v2:
time: 111 us; the launch traced here: 110 us
  Pallas kernels  94.2 us (85%)
  local copies, waits for them, and re-layouts  14.4 us (13%)
    pallas_call x2, Pallas kernels, call(): pl.pallas_call(kernel, out_shape=outs, in_specs=[pl.BlockSpec(memory_spac...  94.2 us
    unnamed x24, local copies, waits for them, and re-layouts  13.3 us

profile of v2, /device:TPU:0, one launch (start us, length us, event | category | flops | bytes accessed | tf_op | source)
XLA Modules:
  0.0 109.6 jit_solution(18136045796282336993)
XLA Ops:
  0.0 0.8 copy.22.extra_ref
  0.8 1.5 %copy.26.weight_ref = f32[256,2]{1,0:T(8,128)} copy(f32[256,2]{0,1:T(2,128)} %param.35) | data formatting | bytes 4096 | tf_op args[17]
  2.3 0.8 copy.23
  3.1 0.1 eq.15
  3.3 0.3 fusion
  3.5 0.1 convert_element_type.10
  3.7 0.1 copy.24
  3.8 0.7 multiply_add_fusion
  4.5 0.0 copy-start.9
  4.5 0.8 copy.25.target_ref
  5.3 0.0 copy-start.1
  5.3 1.6 %copy-done.1 = bf16[512,2048]{1,0:T(8,128)(2,1)S(1)} copy-done((bf16[512,2048]{1,0:T(8,128)(2,1)S(1)}, bf16[512,2048]{1,0:T(8,128)(2,1)}, u32[]{:S(2)}) %copy-start.1) | copy-done | bytes 2097176
  6.9 0.0 copy-start.2
  6.9 0.9 copy-done.2
  7.8 0.0 copy-start.3
  7.8 0.9 copy-done.3
  8.8 0.0 copy-start.4
  8.8 0.9 copy-done.4
  9.7 0.0 copy-start.5
  9.7 0.9 copy-done.5
  10.6 0.0 copy-start.6
  10.6 0.9 copy-done.6
  11.5 0.0 copy-start.7
  11.5 0.7 copy-done.7
  12.2 0.0 copy-start.8
  12.2 0.7 copy-done.8
  12.8 16.4 %shard_map.172.part_ref = bf16[256,2048]{1,0:T(8,128)(2,1)S(1)} custom-call(bf16[256,256]{1,0:T(8,128)(2,1)S(1)} %copy-done.4, bf16[256,256]{1,0:T(8,128)(2,1)S(1)} %copy-done.5, bf16[256,512]{1,0:T(8,128)(2,1)S(1)} %copy-done.2, bf16[256,512]{1,0:T(8,128)(2,1)S(1)} %copy-done.3, bf16[256,256]{1,0:T(8,128)(2,1)S(1)} %copy-done.6, f32[1,256]{1,0:T(1,128)S(1)} %bitcast.9, ...), custom_call_target="tpu_custom_call" | custom-call | tf_op jit(solution)/shard_map/pallas_call | solution.py:518
  29.3 0.0 copy-done.9
  29.3 0.0 copy-start
  29.3 1.0 copy-done
  30.2 77.7 %shard_map.173 = bf16[64,2048]{1,0:T(8,128)(2,1)} custom-call(bf16[256,2048]{1,0:T(8,128)(2,1)} %copy-done, bf16[64,2048]{1,0:T(8,128)(2,1)} %res_hbm.1, f32[1,2048]{1,0:T(1,128)} %bitcast.15, f32[1,2048]{1,0:T(1,128)} %bitcast.16, f32[1,2048]{1,0:T(1,128)} %bitcast.17, s32[256,2]{1,0:T(8,128)} %copy.25.target_ref, s32[2,256]{1,0:T(2,128)} %bitcast.14, ...), custom_call_target="tpu_custom_call" | custom-call | tf_op jit(solution)/shard_map/pallas_call | solution.py:518
  108.0 1.7 %copy.28 = bf16[64,2048]{1,0:T(8,128)(2,1)} copy(bf16[64,2048]{1,0:T(8,128)(2,1)} %shard_map.173) | data formatting | bytes 524288
  (1 shorter events, 0.0 us)
Async XLA Ops:
  4.5 24.8 %copy-start.9 = (s32[256,2]{0,1:T(2,128)}, s32[256,2]{0,1:T(2,128)S(1)}, u32[]{:S(2)}) copy-start(s32[256,2]{0,1:T(2,128)S(1)} %multiply_add_fusion) | copy-start | bytes 6148
  5.3 1.6 %copy-start.1 = (bf16[512,2048]{1,0:T(8,128)(2,1)S(1)}, bf16[512,2048]{1,0:T(8,128)(2,1)}, u32[]{:S(2)}) copy-start(bf16[512,2048]{1,0:T(8,128)(2,1)} %w_hbm.1) | copy-start | bytes 6291460
  6.9 0.9 copy-start.2
  7.8 0.9 copy-start.3
  8.8 0.9 copy-start.4
  9.7 0.9 copy-start.5
  10.6 0.9 copy-start.6
  11.5 0.7 copy-start.7
  12.2 0.7 copy-start.8
  29.3 1.0 copy-start

commit v3 on v2

--- a/solution.py
+++ b/solution.py
@@ -601,7 +601,7 @@
         ]
         + dmas((n_sp,), (n_sp,), (6,)),
         1,
-        32 << 20,
+        67043328,
     )
     hidden_units = expert_gate_weight.shape[2]
     by_peer = (n_sp, n_y)
@@ -651,7 +651,7 @@
             by_peer, by_peer, by_peer, by_peer, (n_sp,), (n_sp,), (n_tp,), (n_tp,),
         ),
         2,
-        56 << 20,
+        67043328,
     )
 
 

time: 111 us -> 105 us (0.946)
  local copies, waits for them, and re-layouts: 14.4 us -> 7.15 us
  Pallas kernels: 94.2 us -> 95.4 us
    unnamed x24 -> x6, local copies, waits for them, and re-layouts: 13.3 us -> 6 us
    pallas_call x2, Pallas kernels: 94.2 us -> 95.4 us  [call(): pl.pallas_call(kernel, out_shape=outs, in_specs=[pl.BlockSpec(memory_spac...]
where the time goes in v3:
time: 105 us; the launch traced here: 104 us
  Pallas kernels  95.4 us (91%)
  local copies, waits for them, and re-layouts  7.15 us (7%)
    pallas_call x2, Pallas kernels, call(): pl.pallas_call(kernel, out_shape=outs, in_specs=[pl.BlockSpec(memory_spac...  95.4 us
    unnamed x6, local copies, waits for them, and re-layouts  6 us

profile of v3, /device:TPU:0, one launch (start us, length us, event | category | flops | bytes accessed | tf_op | source)
XLA Modules:
  0.0 103.5 jit_solution(15299354073143943389)
XLA Ops:
  0.0 1.5 %copy.22.extra_ref = f32[256,4]{1,0:T(8,128)} copy(f32[256,4]{0,1:T(4,128)} %param.24) | data formatting | bytes 8192 | tf_op args[6]
  1.5 1.5 %copy.26.weight_ref = f32[256,2]{1,0:T(8,128)} copy(f32[256,2]{0,1:T(2,128)} %param.35) | data formatting | bytes 4096 | tf_op args[17]
  3.0 0.8 copy.23
  3.8 0.1 eq.15
  3.9 0.3 fusion
  4.2 0.1 convert_element_type.10
  4.3 0.1 copy.24
  4.4 0.7 multiply_add_fusion
  5.1 0.0 copy-start
  5.1 0.6 copy-done
  5.7 0.8 copy.25.target_ref
  6.5 17.6 %shard_map.172.part_ref = bf16[256,2048]{1,0:T(8,128)(2,1)} custom-call(bf16[256,256]{1,0:T(8,128)(2,1)} %q_hbm.1, bf16[256,256]{1,0:T(8,128)(2,1)} %k_hbm.1, bf16[256,512]{1,0:T(8,128)(2,1)} %v_hbm.1, bf16[256,512]{1,0:T(8,128)(2,1)} %g_hbm.1, bf16[256,256]{1,0:T(8,128)(2,1)} %d_hbm.1, f32[1,256]{1,0:T(1,128)} %bitcast.16, f32[256,4]{1,0:T(8,128)} %copy.22.extra_ref, ...), custom_call_target="tpu_custom_call" | custom-call | tf_op jit(solution)/shard_map/pallas_call | solution.py:518
  24.1 77.8 %shard_map.173 = bf16[64,2048]{1,0:T(8,128)(2,1)} custom-call(bf16[256,2048]{1,0:T(8,128)(2,1)} %shard_map.172.part_ref, bf16[64,2048]{1,0:T(8,128)(2,1)} %res_hbm.1, f32[1,2048]{1,0:T(1,128)} %bitcast.13, f32[1,2048]{1,0:T(1,128)} %bitcast.14, f32[1,2048]{1,0:T(1,128)} %bitcast.15, s32[256,2]{1,0:T(8,128)} %copy.25.target_ref, s32[2,256]{1,0:T(2,128)} %bitcast.12, ...), custom_call_target="tpu_custom_call" | custom-call | tf_op jit(solution)/shard_map/pallas_call | solution.py:518
  101.9 1.7 %copy.28 = bf16[64,2048]{1,0:T(8,128)(2,1)} copy(bf16[64,2048]{1,0:T(8,128)(2,1)} %shard_map.173) | data formatting | bytes 524288
  (1 shorter events, 0.0 us)
Async XLA Ops:
  5.1 0.6 copy-start
